TPU v7x, 32 devices: a whole 2x2x4 slice. The times are simulated.
32 devices in a mesh: rep: 4 (over z), fs: 4 (over y, x), tp: 2 (over core).
Axes of the slice: x: 2, y: 2, z: 4, core: 2. Of those that a mesh axis runs over, the one named last changes fastest.
Arguments:
- hidden_in: bfloat16 [2048, 2048], P('rep'), may hold values from -6 to 6
- cotangent: bfloat16 [2048, 2048], P('rep'), may hold values from -3 to 3
- w_up: bfloat16 [2048, 8192], P('rep', ('fs', 'tp')), may hold values from -0.125 to 0.125
- w_down: bfloat16 [8192, 2048], P(('fs', 'tp'), 'rep'), may hold values from -0.0625 to 0.0625
Outputs:
- input_grad: bfloat16 [2048, 2048], P('rep')
- up_grad: float32 [2048, 8192], P('rep', ('fs', 'tp'))
- down_grad: float32 [8192, 2048], P(('fs', 'tp'), 'rep')
All inputs are finite; a program needn't handle non-finite values.
Results may differ from a plain program's by a relative error of at most 0.017.
Values may be sent and summed in bfloat16 or wider, within the bound.
A program may use at most 64 MiB of HBM per device.

v0:
```python
import jax
import jax.numpy as jnp
from jax import lax
from jax.sharding import PartitionSpec as P


def contract_last(left, right):
    return lax.dot_general(
        left, right, (((1,), (1,)), ((), ())), preferred_element_type=jnp.float32
    )


def contract_first(left, right):
    return lax.dot_general(
        left, right, (((0,), (0,)), ((), ())), preferred_element_type=jnp.float32
    )


def on_device(hidden_in, cotangent, w_up, w_down):
    up_full = lax.all_gather(w_up, "rep", axis=0, tiled=True)
    back_grad = contract_last(cotangent, lax.all_gather(w_down, "rep", axis=1, tiled=True))
    preact = jnp.dot(hidden_in, up_full, preferred_element_type=jnp.float32)
    active = jnp.maximum(preact, 0.0)
    hidden = (active * active).astype(jnp.bfloat16)
    slopes = (2.0 * active * back_grad).astype(jnp.bfloat16)
    grad_upper = lax.psum_scatter(
        contract_first(hidden_in, slopes).astype(jnp.bfloat16),
        "rep",
        scatter_dimension=0,
        tiled=True,
    ).astype(jnp.float32)
    lower_rows = lax.psum_scatter(
        contract_first(cotangent, hidden).astype(jnp.bfloat16),
        "rep",
        scatter_dimension=0,
        tiled=True,
    ).astype(jnp.float32)
    down_grad = lower_rows.T
    partial_sum = contract_last(slopes, up_full).astype(jnp.bfloat16)
    input_grad = lax.psum(partial_sum, ("fs", "tp")).astype(jnp.float32).astype(jnp.bfloat16)
    return (input_grad, grad_upper, down_grad)


def solution(mesh):
    return jax.shard_map(
        on_device,
        mesh=mesh,
        in_specs=(P("rep", None), P("rep", None), P("rep", ("fs", "tp")), P(("fs", "tp"), "rep")),
        out_specs=(P("rep", None), P("rep", ("fs", "tp")), P(("fs", "tp"), "rep")),
        check_vma=False,
    )
```

profile of v0, /device:TPU:0, one launch (start us, length us, event | category | flops | bytes accessed | tf_op | source)
XLA Modules:
  0.0 414.7 jit_solution(14841434194789787365)
XLA Ops:
  7.2 0.0 copy-start
  7.2 0.0 all-gather.3.cloned.1.call-start
  7.2 0.7 all-gather.3.cloned.1.call-update
  7.9 0.0 all-gather.5.cloned.1.call-start
  8.0 0.7 all-gather.5.cloned.1.call-update
  8.7 0.0 reduce-scatter.3.cloned.1.call-start
  8.7 84.3 %all-gather.3.cloned.1.call-done = bf16[2048,1024]{1,0:T(8,128)(2,1)} async-done(((bf16[512,1024]{1,0:T(8,128)(2,1)}), bf16[2048,1024]{1,0:T(8,128)(2,1)}) %all-gather.3.cloned.1.call-update) | async-done | bytes 4194320 | tf_op jit(solution)/shard_map/all_gather | solution.py:20
  93.1 0.0 copy-done
  93.1 5.8 %fusion.2 = f32[512,1024]{1,0:T(8,128)} fusion(bf16[512,2048]{1,0:T(8,128)(2,1)S(1)} %copy-done, bf16[2048,1024]{1,0:T(8,128)(2,1)} %all-gather.3.cloned.1.call-done), kind=kOutput, calls=%fused_computation.8 | convolution fusion | flops 2147483648 | bytes 8388608 | tf_op jit(solution)/shard_map/dot_general | solution.py:22
  98.9 75.0 %all-gather.5.cloned.1.call-done = bf16[1024,2048]{1,0:T(8,128)(2,1)} async-done(((bf16[1024,512]{1,0:T(8,128)(2,1)}), bf16[1024,2048]{1,0:T(8,128)(2,1)}) %all-gather.5.cloned.1.call-update) | async-done | bytes 4194320 | tf_op jit(solution)/shard_map/all_gather | solution.py:21
  173.9 5.8 %multiply_convert_fusion.1 = bf16[512,1024]{1,0:T(8,128)(2,1)S(1)} fusion(f32[512,1024]{1,0:T(8,128)} %fusion.2, bf16[512,2048]{1,0:T(8,128)(2,1)} %param.5, bf16[1024,2048]{1,0:T(8,128)(2,1)} %all-gather.5.cloned.1.call-done), kind=kOutput, calls=%fused_computation.5 | convolution fusion | flops 2149580800 | bytes 9437184 | tf_op jit(solution)/shard_map/dot_general | solution.py:8
  179.7 4.4 %convert_bitcast_fusion.1 = bf16[2048,1024]{0,1:T(8,128)(2,1)} fusion(bf16[512,1024]{1,0:T(8,128)(2,1)S(1)} %multiply_convert_fusion.1, bf16[512,2048]{1,0:T(8,128)(2,1)S(1)} %copy-done), kind=kOutput, calls=%fused_computation.1 | convolution fusion | flops 2149580800 | bytes 7340032 | tf_op jit(solution)/shard_map/dot_general | solution.py:14
  184.1 0.0 reduce-scatter.3.cloned.1.call-update
  184.1 0.0 reduce-scatter.5.cloned.1.call-start
  184.2 6.6 %convert_bitcast_fusion = bf16[2048,1024]{0,1:T(8,128)(2,1)} fusion(bf16[512,2048]{1,0:T(8,128)(2,1)} %param.5, f32[512,1024]{1,0:T(8,128)} %fusion.2), kind=kOutput, calls=%fused_computation | convolution fusion | flops 2151153664 | bytes 8388608 | tf_op jit(solution)/shard_map/dot_general | solution.py:14
  190.8 0.0 reduce-scatter.5.cloned.1.call-update
  190.8 0.0 all-reduce.2.cloned.1.call-start
  190.8 5.9 %convolution_convert_fusion = bf16[512,2048]{1,0:T(8,128)(2,1)} fusion(bf16[512,1024]{1,0:T(8,128)(2,1)S(1)} %multiply_convert_fusion.1, bf16[2048,1024]{1,0:T(8,128)(2,1)} %all-gather.3.cloned.1.call-done), kind=kOutput, calls=%fused_computation.2 | convolution fusion | flops 2148532224 | bytes 7340032 | tf_op jit(solution)/shard_map/dot_general | solution.py:8
  196.7 0.0 all-reduce.2.cloned.1.call-update
  196.7 62.8 %reduce-scatter.3.cloned.1.call-done = bf16[512,1024]{0,1:T(8,128)(2,1)} async-done(((bf16[2048,1024]{0,1:T(8,128)(2,1)}), bf16[512,1024]{0,1:T(8,128)(2,1)}) %reduce-scatter.3.cloned.1.call-update) | async-done | bytes 1048592 | tf_op jit(solution)/shard_map/reduce_scatter | solution.py:26
  259.6 2.6 copy.7
  262.1 76.9 %reduce-scatter.5.cloned.1.call-done = bf16[512,1024]{0,1:T(8,128)(2,1)} async-done(((bf16[2048,1024]{0,1:T(8,128)(2,1)}), bf16[512,1024]{0,1:T(8,128)(2,1)}) %reduce-scatter.5.cloned.1.call-update) | async-done | bytes 1048592 | tf_op jit(solution)/shard_map/reduce_scatter | solution.py:32
  339.1 2.8 convert_bitcast_fusion.2
  341.9 63.1 %all-reduce.2.cloned.1.call-done = bf16[512,2048]{1,0:T(8,128)(2,1)} async-done(((bf16[512,2048]{1,0:T(8,128)(2,1)}), bf16[512,2048]{1,0:T(8,128)(2,1)}) %all-reduce.2.cloned.1.call-update) | async-done | bytes 2097168 | tf_op jit(solution)/shard_map/psum | solution.py:40
  405.0 3.2 copy.9
Async XLA Ops:
  7.2 85.9 %copy-start = (bf16[512,2048]{1,0:T(8,128)(2,1)S(1)}, bf16[512,2048]{1,0:T(8,128)(2,1)}, u32[]{:S(2)}) copy-start(bf16[512,2048]{1,0:T(8,128)(2,1)} %param.4) | copy-start | bytes 6291460
  7.2 85.9 %all-gather.3.cloned.1.call-start = ((), (), s32[]{:S(2)}) async-start(), calls=%async_computation.2 | async-start | bytes 5242880 | tf_op jit(solution)/shard_map/all_gather | solution.py:20
  7.9 166.0 %all-gather.5.cloned.1.call-start = ((), (), s32[]{:S(2)}) async-start(), calls=%async_computation.3 | async-start | bytes 5242880 | tf_op jit(solution)/shard_map/all_gather | solution.py:21
  8.7 250.9 %reduce-scatter.3.cloned.1.call-start = ((), (), s32[]{:S(2)}) async-start(), calls=%async_computation.5 | async-start | bytes 5242880 | tf_op jit(solution)/shard_map/reduce_scatter | solution.py:26
  184.1 154.9 %reduce-scatter.5.cloned.1.call-start = ((), (), s32[]{:S(2)}) async-start(), calls=%async_computation.6 | async-start | bytes 5242880 | tf_op jit(solution)/shard_map/reduce_scatter | solution.py:32
  190.8 214.2 %all-reduce.2.cloned.1.call-start = ((), (), s32[]{:S(2)}) async-start(), calls=%async_computation.4 | async-start | bytes 4194304 | tf_op jit(solution)/shard_map/psum | solution.py:40
Sparse Core Ops, SparseCore 0:
  9.6 83.4 all-gather.2
  94.6 79.2 all-gather.4
  184.3 75.2 reduce-scatter.2
  261.7 77.2 reduce-scatter.4
  342.7 62.2 all-reduce.1
where the time goes:
time: 415 us
  waiting for transfers between devices  364 us (88%)
  matrix products  28.5 us (7%)
  between operations  13.8 us (3%)
  local copies, waits for them, and re-layouts  5.73 us (1%)
    all_gather x1, waiting for transfers between devices, on_device(): up_full = lax.all_gather(w_up, 'rep', axis=0, tiled=True)  84.3 us
    reduce_scatter x1, waiting for transfers between devices, on_device(): lax.psum_scatter(contract_first(cotangent, hidden).astype(jnp.bfloat16),...  76.9 us
    all_gather x1, waiting for transfers between devices, on_device(): lax.all_gather(w_down, 'rep', axis=1, tiled=True)  75 us
    psum x1, waiting for transfers between devices, on_device(): lax.psum(partial_sum, ('fs', 'tp')).astype(jnp.float32).astype(jnp.bfloat16)  63.1 us
    reduce_scatter x1, waiting for transfers between devices, on_device(): lax.psum_scatter(contract_first(hidden_in, slopes).astype(jnp.bfloat16),...  62.8 us
    dot_general x2, matrix products, contract_last(): lax.dot_general(left, right, (((1,), (1,)), ((), ())), preferred_element_...  11.7 us
    dot_general x2, matrix products, contract_first(): lax.dot_general(left, right, (((0,), (0,)), ((), ())), preferred_element_...  10.9 us
  transfers between devices with their start and end apart: 5, of which 5 were waited for; matrix products, arithmetic and copies ran while one was open for 6% of the time, Pallas kernels for 0%

commit v1 on v0

--- a/solution.py
+++ b/solution.py
@@ -2,6 +2,17 @@
 import jax.numpy as jnp
 from jax import lax
 from jax.sharding import PartitionSpec as P
+
+
+def pass_along(value, axis, dim):
+    count = lax.axis_size(axis)
+    forward = [(i, (i + 1) % count) for i in range(count)]
+    pieces = [value]
+    for stride in range(1, count):
+        pieces = [lax.ppermute(pieces[0], axis, forward), *pieces]
+    whole = jnp.concatenate(pieces, axis=dim)
+    shift = (lax.axis_index(axis) + 1) * pieces[-1].shape[dim]
+    return jnp.roll(whole, shift, axis=dim)
 
 
 def contract_last(left, right):
@@ -17,7 +28,7 @@
 
 
 def on_device(hidden_in, cotangent, w_up, w_down):
-    up_full = lax.all_gather(w_up, "rep", axis=0, tiled=True)
+    up_full = pass_along(w_up, "rep", 0)
     back_grad = contract_last(cotangent, lax.all_gather(w_down, "rep", axis=1, tiled=True))
     preact = jnp.dot(hidden_in, up_full, preferred_element_type=jnp.float32)
     active = jnp.maximum(preact, 0.0)

time: 415 us -> 400 us (0.964)
  waiting for transfers between devices: 364 us -> 311 us
  starting transfers between devices: 0.2 us -> 32.9 us
  local copies, waits for them, and re-layouts: 5.73 us -> 16.9 us
  matrix products: 28.5 us -> 22.2 us
    ppermute x0 -> x3, waiting for transfers between devices: none -> 110 us  [pass_along(): pieces = [lax.ppermute(pieces[0], axis, forward), *pieces]]
    all_gather x1 -> x0, waiting for transfers between devices: 84.3 us -> none  [on_device(): up_full = lax.all_gather(w_up, 'rep', axis=0, tiled=True)]
    all_gather x1, waiting for transfers between devices: 75 us -> 0.02 us  [on_device(): lax.all_gather(w_down, 'rep', axis=1, tiled=True)]
    ppermute x0 -> x3, starting transfers between devices: none -> 32.6 us  [pass_along(): pieces = [lax.ppermute(pieces[0], axis, forward), *pieces]]
    reduce_scatter x1, waiting for transfers between devices: 76.9 us -> 60.4 us  [on_device(): lax.psum_scatter(contract_first(cotangent, hidden).astype(jnp.bfloat16),...]
    reduce_scatter x1, waiting for transfers between devices: 62.8 us -> 76.8 us  [on_device(): lax.psum_scatter(contract_first(hidden_in, slopes).astype(jnp.bfloat16),...]
    unnamed x4 -> x25, local copies, waits for them, and re-layouts: 5.73 us -> 16.8 us
  transfers between devices with their start and end apart: 5 -> 7, of which waited for: 5 -> 6; matrix products, arithmetic and copies ran while one was open for 6% -> 8% of each run, Pallas kernels for 0% -> 0%
where the time goes in v1:
time: 400 us
  waiting for transfers between devices  311 us (78%)
  starting transfers between devices  32.9 us (8%)
  matrix products  22.2 us (6%)
  local copies, waits for them, and re-layouts  16.9 us (4%)
  between operations  13.9 us (3%)
    ppermute x3, waiting for transfers between devices, pass_along(): pieces = [lax.ppermute(pieces[0], axis, forward), *pieces]  110 us
    reduce_scatter x1, waiting for transfers between devices, on_device(): lax.psum_scatter(contract_first(hidden_in, slopes).astype(jnp.bfloat16),...  76.8 us
    psum x1, waiting for transfers between devices, on_device(): lax.psum(partial_sum, ('fs', 'tp')).astype(jnp.float32).astype(jnp.bfloat16)  63.4 us
    reduce_scatter x1, waiting for transfers between devices, on_device(): lax.psum_scatter(contract_first(cotangent, hidden).astype(jnp.bfloat16),...  60.4 us
    ppermute x3, starting transfers between devices, pass_along(): pieces = [lax.ppermute(pieces[0], axis, forward), *pieces]  32.6 us
    unnamed x25, local copies, waits for them, and re-layouts  16.8 us
    dot_general x2, matrix products, contract_last(): lax.dot_general(left, right, (((1,), (1,)), ((), ())), preferred_element_...  11.3 us
    dot_general x2, matrix products, contract_first(): lax.dot_general(left, right, (((0,), (0,)), ((), ())), preferred_element_...  8.58 us
  transfers between devices with their start and end apart: 7, of which 6 were waited for; matrix products, arithmetic and copies ran while one was open for 8% of the time, Pallas kernels for 0%

profile of v1, /device:TPU:0, one launch (start us, length us, event | category | flops | bytes accessed | tf_op | source)
XLA Modules:
  0.0 399.7 jit_solution(14834524753716908037)
XLA Ops:
  7.2 0.0 copy-start
  7.2 0.0 copy-start.1
  7.2 0.0 all-gather.2.cloned.1.call-start
  7.2 0.7 all-gather.2.cloned.1.call-update
  7.9 0.0 reduce-scatter.5.cloned.1.call-start
  8.0 3.1 collective-permute-start
  11.1 37.6 %collective-permute-done = bf16[512,1024]{1,0:T(8,128)(2,1)S(1)} collective-permute-done((bf16[512,1024]{1,0:T(8,128)(2,1)}, bf16[512,1024]{1,0:T(8,128)(2,1)S(1)}, u32[]{:S(2)}, u32[]{:S(2)}) %collective-permute-start) | collective-permute-done | bytes 1048608 | tf_op jit(solution)/shard_map/ppermute | solution.py:12
  48.7 0.0 copy-start.2
  48.7 1.0 copy-done.2
  49.7 14.7 %collective-permute-start.1 = (bf16[512,1024]{1,0:T(8,128)(2,1)S(1)}, bf16[512,1024]{1,0:T(8,128)(2,1)}, u32[]{:S(2)}, u32[]{:S(2)}) collective-permute-start(bf16[512,1024]{1,0:T(8,128)(2,1)S(1)} %collective-permute-done), channel_id=1, source_target_pairs={{0,8},{8,16},{16,24},{24,0},{1,9},{9,17},{17,25},{25,1},{2,10},{10... | collective-permute-start | bytes 3145736 | tf_op jit(solution)/shard_map/ppermute | solution.py:12
  64.4 46.0 %collective-permute-done.1 = bf16[512,1024]{1,0:T(8,128)(2,1)} collective-permute-done((bf16[512,1024]{1,0:T(8,128)(2,1)S(1)}, bf16[512,1024]{1,0:T(8,128)(2,1)}, u32[]{:S(2)}, u32[]{:S(2)}) %collective-permute-start.1) | collective-permute-done | bytes 1048608 | tf_op jit(solution)/shard_map/ppermute | solution.py:12
  110.4 14.7 %collective-permute-start.2 = (bf16[512,1024]{1,0:T(8,128)(2,1)}, bf16[512,1024]{1,0:T(8,128)(2,1)}, u32[]{:S(2)}, u32[]{:S(2)}) collective-permute-start(bf16[512,1024]{1,0:T(8,128)(2,1)} %collective-permute-done.1), channel_id=1, source_target_pairs={{0,8},{8,16},{16,24},{24,0},{1,9},{9,17},{17,25},{25,1},{2,10},{10... | collective-permute-start | bytes 3145736 | tf_op jit(solution)/shard_map/ppermute | solution.py:12
  125.2 0.0 copy-start.3
  125.2 25.9 %collective-permute-done.2 = bf16[512,1024]{1,0:T(8,128)(2,1)} collective-permute-done((bf16[512,1024]{1,0:T(8,128)(2,1)}, bf16[512,1024]{1,0:T(8,128)(2,1)}, u32[]{:S(2)}, u32[]{:S(2)}) %collective-permute-start.2) | collective-permute-done | bytes 1048608 | tf_op jit(solution)/shard_map/ppermute | solution.py:12
  151.1 1.3 constant_dynamic-update-slice_fusion.7
  152.4 1.3 constant_dynamic-update-slice_fusion.6
  153.7 0.0 copy-done.3
  153.7 0.1 constant_dynamic-update-slice_fusion.5
  153.8 0.0 copy-done.1
  153.8 0.1 constant_dynamic-update-slice_fusion.4
  153.8 0.0 copy-start.5
  153.9 1.4 constant_dynamic-update-slice_fusion.3
  155.3 1.3 constant_dynamic-update-slice_fusion.2
  156.6 0.1 constant_dynamic-update-slice_fusion.1
  156.7 0.1 constant_dynamic-update-slice_fusion
  156.8 0.0 copy-start.4
  156.8 3.2 copy-done.4
  160.0 0.0 copy-done.5
  160.0 2.4 fusion.2
  162.4 0.0 copy-start.7
  162.4 1.3 copy-done.7
  163.7 0.0 copy-done
  163.7 4.3 %convert_bitcast_fusion = bf16[2048,1024]{0,1:T(8,128)(2,1)} fusion(bf16[512,2048]{1,0:T(8,128)(2,1)S(1)} %copy-done, f32[1024,512]{1,0:T(8,128)S(1)} %fusion.2), kind=kOutput, calls=%fused_computation | convolution fusion | flops 2151153664 | bytes 8388608 | tf_op jit(solution)/shard_map/dot_general | solution.py:25
  168.0 0.0 reduce-scatter.5.cloned.1.call-update
  168.0 0.0 reduce-scatter.3.cloned.1.call-start
  168.0 0.0 all-gather.2.cloned.1.call-done
  168.1 0.0 copy-start.6
  168.1 5.4 %fusion.7 = bf16[512,1024]{0,1:T(8,128)(2,1)S(1)} fusion(f32[1024,512]{1,0:T(8,128)} %copy-done.7, bf16[512,2048]{1,0:T(8,128)(2,1)S(1)} %copy-done, bf16[1024,2048]{1,0:T(8,128)(2,1)} %all-gather.2.cloned.1.call-done), kind=kOutput, calls=%fused_computation.8 | convolution fusion | flops 2149580800 | bytes 9437184 | tf_op jit(solution)/shard_map/dot_general | solution.py:19
  173.5 0.0 copy-done.6
  173.5 4.3 %convert_bitcast_fusion.1 = bf16[2048,1024]{0,1:T(8,128)(2,1)} fusion(bf16[512,1024]{0,1:T(8,128)(2,1)S(1)} %fusion.7, bf16[512,2048]{1,0:T(8,128)(2,1)S(1)} %copy-done.6), kind=kOutput, calls=%fused_computation.1 | convolution fusion | flops 2149580800 | bytes 7340032 | tf_op jit(solution)/shard_map/dot_general | solution.py:25
  177.8 0.0 reduce-scatter.3.cloned.1.call-update
  177.8 0.2 all-reduce.2.cloned.1.call-start
  178.0 5.9 %fusion.4 = bf16[512,2048]{1,0:T(8,128)(2,1)} fusion(bf16[512,1024]{0,1:T(8,128)(2,1)S(1)} %fusion.7, bf16[4096,1024]{1,0:T(8,128)(2,1)} %copy-done.4, s32[]{:T(128)S(6)} %select_n.14), kind=kOutput, calls=%fused_computation.6 | convolution fusion | flops 2148532224 | bytes 7340036 | tf_op jit(solution)/shard_map/dot_general | solution.py:19
  183.9 0.0 all-reduce.2.cloned.1.call-update
  183.9 60.4 %reduce-scatter.5.cloned.1.call-done = bf16[512,1024]{0,1:T(8,128)(2,1)} async-done(((bf16[2048,1024]{0,1:T(8,128)(2,1)}), bf16[512,1024]{0,1:T(8,128)(2,1)}) %reduce-scatter.5.cloned.1.call-update) | async-done | bytes 1048592 | tf_op jit(solution)/shard_map/reduce_scatter | solution.py:43
  244.4 2.8 convert_bitcast_fusion.2
  247.2 76.8 %reduce-scatter.3.cloned.1.call-done = bf16[512,1024]{0,1:T(8,128)(2,1)} async-done(((bf16[2048,1024]{0,1:T(8,128)(2,1)}), bf16[512,1024]{0,1:T(8,128)(2,1)}) %reduce-scatter.3.cloned.1.call-update) | async-done | bytes 1048592 | tf_op jit(solution)/shard_map/reduce_scatter | solution.py:37
  324.0 2.6 copy.8
  326.6 63.4 %all-reduce.2.cloned.1.call-done = bf16[512,2048]{1,0:T(8,128)(2,1)} async-done(((bf16[512,2048]{1,0:T(8,128)(2,1)}), bf16[512,2048]{1,0:T(8,128)(2,1)}) %all-reduce.2.cloned.1.call-update) | async-done | bytes 2097168 | tf_op jit(solution)/shard_map/psum | solution.py:51
  390.0 3.2 copy.18
Async XLA Ops:
  7.2 156.5 %copy-start = (bf16[512,2048]{1,0:T(8,128)(2,1)S(1)}, bf16[512,2048]{1,0:T(8,128)(2,1)}, u32[]{:S(2)}) copy-start(bf16[512,2048]{1,0:T(8,128)(2,1)} %param.5) | copy-start | bytes 6291460
  7.2 146.6 %copy-start.1 = (bf16[512,1024]{1,0:T(8,128)(2,1)S(1)}, bf16[512,1024]{1,0:T(8,128)(2,1)}, u32[]{:S(2)}) copy-start(bf16[512,1024]{1,0:T(8,128)(2,1)} %param.6) | copy-start | bytes 3145732
  7.2 160.9 %all-gather.2.cloned.1.call-start = ((), (), s32[]{:S(2)}) async-start(), calls=%async_computation.2 | async-start | bytes 5242880 | tf_op jit(solution)/shard_map/all_gather | solution.py:32
  7.9 236.5 %reduce-scatter.5.cloned.1.call-start = ((), (), s32[]{:S(2)}) async-start(), calls=%async_computation.5 | async-start | bytes 5242880 | tf_op jit(solution)/shard_map/reduce_scatter | solution.py:43
  8.0 40.7 %collective-permute-start = (bf16[512,1024]{1,0:T(8,128)(2,1)}, bf16[512,1024]{1,0:T(8,128)(2,1)S(1)}, u32[]{:S(2)}, u32[]{:S(2)}) collective-permute-start(bf16[512,1024]{1,0:T(8,128)(2,1)} %param.6), channel_id=1, source_target_pairs={{0,8},{8,16},{16,24},{24,0},{1,9},{9,17},{17,25},{25,1},{2,10},{10... | collective-permute-start | bytes 3145736 | tf_op jit(solution)/shard_map/ppermute | solution.py:12
  48.7 1.0 copy-start.2
  49.7 60.8 %collective-permute-start.1 = (bf16[512,1024]{1,0:T(8,128)(2,1)S(1)}, bf16[512,1024]{1,0:T(8,128)(2,1)}, u32[]{:S(2)}, u32[]{:S(2)}) collective-permute-start(bf16[512,1024]{1,0:T(8,128)(2,1)S(1)} %collective-permute-done), channel_id=1, source_target_pairs={{0,8},{8,16},{16,24},{24,0},{1,9},{9,17},{17,25},{25,1},{2,10},{10... | collective-permute-start | bytes 3145736 | tf_op jit(solution)/shard_map/ppermute | solution.py:12
  110.4 40.6 %collective-permute-start.2 = (bf16[512,1024]{1,0:T(8,128)(2,1)}, bf16[512,1024]{1,0:T(8,128)(2,1)}, u32[]{:S(2)}, u32[]{:S(2)}) collective-permute-start(bf16[512,1024]{1,0:T(8,128)(2,1)} %collective-permute-done.1), channel_id=1, source_target_pairs={{0,8},{8,16},{16,24},{24,0},{1,9},{9,17},{17,25},{25,1},{2,10},{10... | collective-permute-start | bytes 3145736 | tf_op jit(solution)/shard_map/ppermute | solution.py:12
  125.2 28.5 %copy-start.3 = (bf16[512,1024]{1,0:T(8,128)(2,1)S(1)}, bf16[512,1024]{1,0:T(8,128)(2,1)}, u32[]{:S(2)}) copy-start(bf16[512,1024]{1,0:T(8,128)(2,1)} %copy-done.2) | copy-start | bytes 3145732
  153.8 6.1 %copy-start.5 = (bf16[512,2048]{1,0:T(8,128)(2,1)S(1)}, bf16[512,2048]{1,0:T(8,128)(2,1)}, u32[]{:S(2)}) copy-start(bf16[512,2048]{1,0:T(8,128)(2,1)} %param.4) | copy-start | bytes 6291460
  156.8 3.2 copy-start.4
  162.4 1.3 copy-start.7
  168.0 156.0 %reduce-scatter.3.cloned.1.call-start = ((), (), s32[]{:S(2)}) async-start(), calls=%async_computation.4 | async-start | bytes 5242880 | tf_op jit(solution)/shard_map/reduce_scatter | solution.py:37
  168.1 5.4 %copy-start.6 = (bf16[512,2048]{1,0:T(8,128)(2,1)S(1)}, bf16[512,2048]{1,0:T(8,128)(2,1)}, u32[]{:S(2)}) copy-start(bf16[512,2048]{1,0:T(8,128)(2,1)} %param.4) | copy-start | bytes 6291460
  177.8 212.2 %all-reduce.2.cloned.1.call-start = ((), (), s32[]{:S(2)}) async-start(), calls=%async_computation.3 | async-start | bytes 4194304 | tf_op jit(solution)/shard_map/psum | solution.py:51
Sparse Core Ops, SparseCore 0:
  9.6 117.3 all-gather.1
  168.1 76.2 reduce-scatter.4
  246.7 77.2 reduce-scatter.2
  327.7 62.2 all-reduce.1
